TPU v7x, 32 devices: a whole 2x2x4 slice. The times are simulated.
32 devices in a mesh: grp: 2 (over x), tp: 16 (over z, y, core).
Axes of the slice: x: 2, y: 2, z: 4, core: 2. Of those that a mesh axis runs over, the one named last changes fastest.
Arguments:
- tokens: bfloat16 [2048, 2048], P('grp', 'tp'), parts along dimension 0, may hold values from -8 to 8
- carried: float32 [2, 2, 32, 64, 2048], P(None, None, 'tp', None, 'grp'), parts along dimension 4, may hold values from -3 to 3
- proj_in: bfloat16 [2, 2048, 512], P(None, None, 'tp'), may hold values from -0.125 to 0.125
- proj_gate: bfloat16 [2, 2048, 512], P(None, None, 'tp'), may hold values from -0.125 to 0.125
- proj_out: bfloat16 [2, 512, 2048], P(None, None, 'tp'), may hold values from -0.5 to 0.5
- norm_params: bfloat16 [2, 2, 2048], P(None, None, 'tp'), may hold values from -0.5 to 2.4
- lambda_re: float32 [2, 32, 64], P(None, 'tp'), may hold values from -1 to -0.05
- lambda_im: float32 [2, 32, 64], P(None, 'tp'), may hold values from -3 to 3
- log_step: float32 [2, 32], P(None, 'tp'), may hold values from -3 to 0
- in_coupling: float32 [2, 2, 32, 64, 16], P(None, None, 'tp'), may hold values from -1 to 1
- out_coupling: float32 [2, 2, 32, 16, 64], P(None, None, 'tp'), may hold values from -1.5 to 1.5
- skip_gain: float32 [2, 512], P(None, 'tp'), may hold values from -4 to 4
Outputs:
- stream_out: bfloat16 [2048, 2048], P('grp', 'tp'), parts along dimension 0
- new_carried: float32 [2, 2, 32, 64, 2048], P(None, None, 'tp', None, 'grp'), parts along dimension 4
There are 2 independent parts, one for each index of `grp`. A program takes and returns all parts, laid end to end along the dimension named above; an argument that names none is the same for every part. Nothing has to cross between parts.
All inputs are finite; a program needn't handle non-finite values.
Results may differ from a plain program's by a relative error of at most 0.015.
Values may be sent and summed in bfloat16 or wider, within the bound.
A program may use at most 64 MiB of HBM per device.

v0:
```python
import jax
import jax.numpy as jnp
from jax import lax
from jax.sharding import PartitionSpec as P

residual_scale = 1.4142135623730951
norm_eps = 1e-05
highest_precision = lax.Precision.HIGHEST


def discretize(lam_re, lam_im, log_dt, coupling):
    step_len = jnp.exp(log_dt)[:, None]
    modulus = jnp.exp(lam_re * step_len)
    decay_re = modulus * jnp.cos(lam_im * step_len)
    decay_im = modulus * jnp.sin(lam_im * step_len)
    denominator = lam_re * lam_re + lam_im * lam_im
    shifted = decay_re - 1.0
    coef_re = (shifted * lam_re + decay_im * lam_im) / denominator
    coef_im = (decay_im * lam_re - shifted * lam_im) / denominator
    in_re = coef_re[..., None] * coupling[0] - coef_im[..., None] * coupling[1]
    in_im = coef_re[..., None] * coupling[1] + coef_im[..., None] * coupling[0]
    return (decay_re, decay_im, in_re, in_im)


def recur(drive, gate_pre, states, lam_re, lam_im, log_dt, in_c, output_coupling, skip_connection):
    channel_groups = lam_re.shape[0]
    batch_rows = drive.shape[0]
    drive_expanded = drive.astype(jnp.float32).reshape(batch_rows, channel_groups, -1)
    decay_re, decay_im, in_re, in_im = discretize(lam_re, lam_im, log_dt, in_c)
    push_re = jnp.einsum("bgc,gpc->gpb", drive_expanded, in_re, precision=highest_precision)
    push_im = jnp.einsum("bgc,gpc->gpb", drive_expanded, in_im, precision=highest_precision)
    fresh_real = decay_re[..., None] * states[0] - decay_im[..., None] * states[1] + push_re
    fresh_imaginary = decay_re[..., None] * states[1] + decay_im[..., None] * states[0] + push_im
    readout_rows = (
        jnp.einsum("jyn,jmy->njm", fresh_real, output_coupling[0], precision=highest_precision)
        - jnp.einsum(
            "jyn,jmy->njm", fresh_imaginary, output_coupling[1], precision=highest_precision
        )
        + skip_connection.reshape(channel_groups, -1) * drive_expanded
    )
    readout_rows = readout_rows.reshape(batch_rows, -1)
    gated = (jax.nn.gelu(readout_rows) * jax.nn.sigmoid(gate_pre.astype(jnp.float32))).astype(
        jnp.bfloat16
    )
    return (gated, jnp.stack([fresh_real, fresh_imaginary]))


def norm_whole(summed, params):
    wide = summed.astype(jnp.float32)
    mean_row = jnp.mean(wide, axis=-1, keepdims=True)
    var_row = jnp.mean(wide * wide, axis=-1, keepdims=True) - mean_row * mean_row
    scaled = (wide - mean_row) * lax.rsqrt(var_row + norm_eps)
    return (scaled * params[0].astype(jnp.float32) + params[1].astype(jnp.float32)).astype(
        jnp.bfloat16
    )


def per_device(
    tokens,
    carried,
    proj_in,
    proj_gate,
    proj_out,
    norm_params,
    lambda_re,
    lambda_im,
    log_step,
    in_coupling,
    out_coupling,
    skip_gain,
):
    layer_count = proj_in.shape[0]
    width_dev = tokens.shape[1]
    out_whole, params_whole = (
        lax.all_gather(proj_out, "tp", axis=2, tiled=True),
        lax.all_gather(norm_params, "tp", axis=2, tiled=True),
    )
    whole_rows = lax.all_gather(tokens, "tp", axis=1, tiled=True)
    new_states = []
    for layer_idx in range(layer_count):
        drive = jnp.dot(whole_rows, proj_in[layer_idx], preferred_element_type=jnp.float32).astype(
            jnp.bfloat16
        )
        gate_pre = jnp.dot(
            whole_rows, proj_gate[layer_idx], preferred_element_type=jnp.float32
        ).astype(jnp.bfloat16)
        gated, states = recur(
            drive,
            gate_pre,
            carried[layer_idx],
            lambda_re[layer_idx],
            lambda_im[layer_idx],
            log_step[layer_idx],
            in_coupling[layer_idx],
            out_coupling[layer_idx],
            skip_gain[layer_idx],
        )
        gated_all = lax.all_gather(gated, "tp", axis=1, tiled=True)
        mixed = jnp.dot(gated_all, out_whole[layer_idx], preferred_element_type=jnp.float32)
        summed = (residual_scale * whole_rows.astype(jnp.float32) + mixed).astype(jnp.bfloat16)
        whole_rows = norm_whole(summed, params_whole[layer_idx])
        new_states.append(states)
    own_cols = lax.dynamic_slice_in_dim(whole_rows, lax.axis_index("tp") * width_dev, width_dev, 1)
    return (own_cols, jnp.stack(new_states))


def solution(mesh):
    return jax.shard_map(
        per_device,
        mesh=mesh,
        in_specs=(
            P("grp", "tp"),
            P(None, None, "tp", None, "grp"),
            P(None, None, "tp"),
            P(None, None, "tp"),
            P(None, None, "tp"),
            P(None, None, "tp"),
            P(None, "tp", None),
            P(None, "tp", None),
            P(None, "tp"),
            P(None, None, "tp", None, None),
            P(None, None, "tp", None, None),
            P(None, "tp"),
        ),
        out_specs=(P("grp", "tp"), P(None, None, "tp", None, "grp")),
        check_vma=False,
    )
```

profile of v0, /device:TPU:0, one launch (start us, length us, event | category | flops | bytes accessed | tf_op | source)
XLA Modules:
  0.0 223.9 jit_solution(7766743840386946516)
XLA Ops:
  7.2 0.0 copy-start.2
  7.2 0.0 all-gather.5.cloned.1.call-start
  7.2 0.7 all-gather.5.cloned.1.call-update
  7.9 0.0 all-gather.9.cloned.1.call-start
  8.0 0.7 all-gather.9.cloned.1.call-update
  8.7 0.0 all-gather.7.cloned.1.call-start
  8.7 1.2 slice_reduce_fusion
  10.0 0.6 mul.485
  10.6 0.8 exponential_bitcast_fusion
  11.4 1.4 fusion.89
  12.7 1.3 fusion.95
  14.0 0.7 fusion.98
  14.8 50.6 %all-gather.5.cloned.1.call-done = bf16[1024,2048]{1,0:T(8,128)(2,1)} async-done(((bf16[1024,128]{1,0:T(8,128)(2,1)}), bf16[1024,2048]{1,0:T(8,128)(2,1)}) %all-gather.5.cloned.1.call-update) | async-done | bytes 4194320 | tf_op jit(solution)/shard_map/all_gather | solution.py:78
  65.4 3.7 %convolution_convert_fusion.3 = bf16[1024,32]{0,1:T(8,128)(2,1)S(1)} fusion(bf16[1024,2048]{1,0:T(8,128)(2,1)} %all-gather.5.cloned.1.call-done, bf16[2,2048,32]{1,2,0:T(8,128)(2,1)} %param.14), kind=kOutput, calls=%fused_computation.28 | convolution fusion | flops 134250496 | bytes 4390912 | tf_op jit(solution)/shard_map/dot_general | solution.py:81
  69.1 0.0 copy-done.6
  69.1 0.5 convolution_add_fusion.3
  69.6 0.4 fusion.62
  70.0 1.1 convolution_add_fusion.2
  71.2 0.4 fusion.9
  71.6 2.0 fusion.16
  73.6 0.0 all-gather.7.cloned.1.call-update
  73.7 0.0 all-gather.11.cloned.1.call-start
  73.7 0.7 mul.523
  74.4 19.0 %all_gather.18 = bf16[2,2,2048]{2,1,0:T(2,128)(2,1)S(1)} all-gather(bf16[2,2,128]{2,1,0:T(2,128)(2,1)} %param.17), channel_id=1, replica_groups=mesh['grp'=2,'tp'=16] {'tp'}, dimensions={2}, use_global_device_ids=true | all-gather | bytes 17408 | tf_op jit(solution)/shard_map/all_gather | solution.py:76
  93.4 24.9 %all-gather.9.cloned.1.call-done = bf16[2,512,2048]{2,1,0:T(8,128)(2,1)} async-done(((bf16[2,512,128]{2,1,0:T(8,128)(2,1)}), bf16[2,512,2048]{2,1,0:T(8,128)(2,1)}) %all-gather.9.cloned.1.call-update) | async-done | bytes 4194320 | tf_op jit(solution)/shard_map/all_gather | solution.py:75
  118.3 38.8 %all-gather.7.cloned.1.call-done = bf16[1024,512]{0,1:T(8,128)(2,1)} async-done(((bf16[1024,32]{0,1:T(8,128)(2,1)}), bf16[1024,512]{0,1:T(8,128)(2,1)}) %all-gather.7.cloned.1.call-update) | async-done | bytes 1048592 | tf_op jit(solution)/shard_map/all_gather | solution.py:98
  157.1 6.6 %convert_reduce_fusion = (f32[1024]{0:T(1024)S(1)}, f32[1024]{0:T(1024)S(1)}, bf16[1024,2048]{1,0:T(8,128)(2,1)S(1)}) fusion(bf16[1024,512]{0,1:T(8,128)(2,1)} %all-gather.7.cloned.1.call-done, bf16[2,512,2048]{2,1,0:T(8,128)(2,1)} %all-gather.9.cloned.1.call-done, bf16[1024,2048]{1,0:T(8,128)(2,1)} %all-gather.5.cloned.1.call-done), kind=kOutput, calls=%fused_computation.2 | convolution fusion | flops 2164258816 | bytes 11542528 | tf_op jit(solution)/shard_map/dot_general | solution.py:99
  163.7 0.0 copy-start.4
  163.8 1.9 fusion.3
  165.6 0.0 copy-start.3
  165.7 0.0 copy-start.9
  165.7 0.0 copy-start.10
  165.7 1.3 convolution_convert_fusion.1
  167.0 1.7 copy-done.3
  168.8 0.5 convolution_add_fusion
  169.2 0.5 convolution_add_fusion.1
  169.7 0.4 fusion.55
  170.1 0.4 fusion.7
  170.5 2.0 fusion.23
  172.5 0.0 all-gather.11.cloned.1.call-update
  172.6 0.1 dynamic-slice
  172.7 0.1 dynamic-slice.1
  172.7 0.1 maximum_bitcast_fusion
  172.8 0.1 maximum_bitcast_fusion.1
  172.9 1.5 pad_maximum_fusion
  174.3 35.2 %all-gather.11.cloned.1.call-done = bf16[1024,512]{0,1:T(8,128)(2,1)} async-done(((bf16[1024,32]{0,1:T(8,128)(2,1)}), bf16[1024,512]{0,1:T(8,128)(2,1)}) %all-gather.11.cloned.1.call-update) | async-done | bytes 1048592 | tf_op jit(solution)/shard_map/all_gather | solution.py:98
  209.5 6.7 %fusion.100 = (f32[1024]{0:T(1024)S(1)}, f32[1024]{0:T(1024)S(1)}, f32[1024,2048]{1,0:T(8,128)S(1)}) fusion(bf16[1024,512]{0,1:T(8,128)(2,1)} %all-gather.11.cloned.1.call-done, bf16[2,512,2048]{2,1,0:T(8,128)(2,1)} %all-gather.9.cloned.1.call-done, bf16[1024,2048]{1,0:T(8,128)(2,1)} %copy-done), kind=kOutput, calls=%fused_computation.168 | convolution fusion | flops 2164258816 | bytes 15736832 | tf_op jit(solution)/shard_map/dot_general | solution.py:99
  216.3 1.1 fusion.27
  (22 shorter events, 0.1 us)
Async XLA Ops:
  7.2 61.9 %copy-start.6 = (f32[2,2,2,64,16]{3,4,2,1,0:T(8,128)S(1)}, f32[2,2,2,64,16]{3,4,2,1,0:T(8,128)}, u32[]{:S(2)}) copy-start(f32[2,2,2,64,16]{3,4,2,1,0:T(8,128)} %param.21) | copy-start | bytes 98308
  7.2 61.9 %copy-start.2 = (f32[2,2,2,64,1024]{4,3,2,1,0:T(8,128)S(1)}, f32[2,2,2,64,1024]{4,3,2,1,0:T(8,128)}, u32[]{:S(2)}) copy-start(f32[2,2,2,64,1024]{4,3,2,1,0:T(8,128)} %param.13) | copy-start | bytes 6291460
  7.2 62.5 %copy-start.7 = (f32[2,2,2,16,64]{4,3,2,1,0:T(8,128)S(1)}, f32[2,2,2,16,64]{4,3,2,1,0:T(8,128)}, u32[]{:S(2)}) copy-start(f32[2,2,2,16,64]{4,3,2,1,0:T(8,128)} %param.22) | copy-start | bytes 98308
  7.2 58.2 %all-gather.5.cloned.1.call-start = ((), (), s32[]{:S(2)}) async-start(), calls=%async_computation | async-start | bytes 4456448 | tf_op jit(solution)/shard_map/all_gather | solution.py:78
  7.9 110.4 %all-gather.9.cloned.1.call-start = ((), (), s32[]{:S(2)}) async-start(), calls=%async_computation.2 | async-start | bytes 4456448 | tf_op jit(solution)/shard_map/all_gather | solution.py:75
  8.7 148.4 %all-gather.7.cloned.1.call-start = ((), (), s32[]{:S(2)}) async-start(), calls=%async_computation.1 | async-start | bytes 1114112 | tf_op jit(solution)/shard_map/all_gather | solution.py:98
  14.0 55.6 %copy-start.11 = (f32[2,64]{1,0:T(2,128)}, f32[2,64]{1,0:T(2,128)S(1)}, u32[]{:S(2)}) copy-start(f32[2,64]{1,0:T(2,128)S(1)} %get-tuple-element.11) | copy-start | bytes 1540
  14.7 54.9 %copy-start.8 = (f32[2,64]{1,0:T(2,128)}, f32[2,64]{1,0:T(2,128)S(1)}, u32[]{:S(2)}) copy-start(f32[2,64]{1,0:T(2,128)S(1)} %fusion.98) | copy-start | bytes 1540
  14.7 56.9 %copy-start.5 = (bf16[2,2048,32]{1,2,0:T(8,128)(2,1)S(1)}, bf16[2,2048,32]{1,2,0:T(8,128)(2,1)}, u32[]{:S(2)}) copy-start(bf16[2,2048,32]{1,2,0:T(8,128)(2,1)} %param.15) | copy-start | bytes 786436
  65.4 5.8 %copy-start.12 = (f32[2,16]{1,0:T(2,128)S(1)}, f32[2,16]{1,0:T(2,128)}, u32[]{:S(2)}) copy-start(f32[2,16]{1,0:T(2,128)} %mul.485) | copy-start | bytes 388
  65.4 6.2 %copy-start.1 = (bf16[1024,2048]{1,0:T(8,128)(2,1)S(1)}, bf16[1024,2048]{1,0:T(8,128)(2,1)}, u32[]{:S(2)}) copy-start(bf16[1024,2048]{1,0:T(8,128)(2,1)} %all-gather.5.cloned.1.call-done) | copy-start | bytes 12582916
  73.7 135.9 %all-gather.11.cloned.1.call-start = ((), (), s32[]{:S(2)}) async-start(), calls=%async_computation.3 | async-start | bytes 1114112 | tf_op jit(solution)/shard_map/all_gather | solution.py:98
  163.7 1.9 copy-start.4
  165.6 4.9 %copy-start = (bf16[1024,2048]{1,0:T(8,128)(2,1)}, bf16[1024,2048]{1,0:T(8,128)(2,1)S(1)}, u32[]{:S(2)}) copy-start(bf16[1024,2048]{1,0:T(8,128)(2,1)S(1)} %fusion.3) | copy-start | bytes 12582916
  165.6 3.1 %copy-start.3 = (f32[2,2,2,64,1024]{4,3,2,1,0:T(8,128)S(1)}, f32[2,2,2,64,1024]{4,3,2,1,0:T(8,128)}, u32[]{:S(2)}) copy-start(f32[2,2,2,64,1024]{4,3,2,1,0:T(8,128)} %param.13) | copy-start | bytes 6291460
  165.7 3.1 %copy-start.9 = (f32[2,64]{1,0:T(2,128)S(1)}, f32[2,64]{1,0:T(2,128)}, u32[]{:S(2)}) copy-start(f32[2,64]{1,0:T(2,128)} %get-tuple-element.8) | copy-start | bytes 1540
  165.7 3.1 %copy-start.10 = (f32[2,64]{1,0:T(2,128)S(1)}, f32[2,64]{1,0:T(2,128)}, u32[]{:S(2)}) copy-start(f32[2,64]{1,0:T(2,128)} %get-tuple-element.20) | copy-start | bytes 1540
Sparse Core Ops, SparseCore 0:
  10.2 55.1 all-gather.4
  67.5 50.7 all-gather.8
  121.0 36.0 all-gather.6
  172.7 36.8 all-gather.10
where the time goes:
time: 224 us
  waiting for transfers between devices  151 us (67%)
  matrix products  26.5 us (12%)
  blocking collectives  19 us (8%)
  between operations  14 us (6%)
  other arithmetic  7.94 us (4%)
  local copies, waits for them, and re-layouts  5.24 us (2%)
    all_gather x2, waiting for transfers between devices, per_device(): gated_all = lax.all_gather(gated, 'tp', axis=1, tiled=True)  74 us
    all_gather x1, waiting for transfers between devices, per_device(): whole_rows = lax.all_gather(tokens, 'tp', axis=1, tiled=True)  50.6 us
    all_gather x1, waiting for transfers between devices, per_device(): lax.all_gather(proj_out, 'tp', axis=2, tiled=True)  24.9 us
    all_gather x1, blocking collectives, per_device(): lax.all_gather(norm_params, 'tp', axis=2, tiled=True)  19 us
    dot_general x2, matrix products, per_device(): jnp.dot(gated_all, out_whole[layer_idx], preferred_element_type=jnp.float32)  13.3 us
    dot_general x2, matrix products, per_device(): jnp.dot(whole_rows, proj_in[layer_idx], preferred_element_type=jnp.float32)  5 us
  transfers between devices with their start and end apart: 4, of which 4 were waited for; matrix products, arithmetic and copies ran while one was open for 7% of the time, Pallas kernels for 0%

commit v1 on v0

v1 whole, which is shorter than its diff:
```python
import functools

import jax
import jax.numpy as jnp
from jax import lax
from jax.experimental import pallas as pl
from jax.experimental.pallas import tpu as pltpu
from jax.sharding import PartitionSpec as P

RESIDUAL_SCALE = 1.4142135623730951
NORM_EPS = 1e-05
HIGHEST = lax.Precision.HIGHEST
F32 = jnp.float32
BF16 = jnp.bfloat16


def column(row):
    m = row.shape[1]
    eye = lax.broadcasted_iota(jnp.int32, (m, m), 0) == lax.broadcasted_iota(jnp.int32, (m, m), 1)
    return jnp.sum(jnp.where(eye, jnp.broadcast_to(row, (m, m)), 0.0), axis=1, keepdims=True)


class Gather:
    def __init__(self, buf, send, recv, place, outer):
        self.buf, self.send, self.recv, self.outer = buf, send, recv, outer
        self.z, self.y, self.c = place

    def idx(self, dz, dy, dc):
        z = lax.rem(self.z + dz + self.outer, self.outer)
        y = self.y if dy == 0 else 1 - self.y
        c = self.c if dc == 0 else 1 - self.c
        return (z * 2 + y) * 2 + c

    def copy(self, block, target, slot):
        return pltpu.make_async_remote_copy(
            src_ref=self.buf.at[block],
            dst_ref=self.buf.at[block],
            send_sem=self.send.at[slot],
            recv_sem=self.recv.at[slot],
            device_id={"tp": target},
            device_id_type=pl.DeviceIdType.MESH,
        )

    def out_z(self, dz):
        return self.copy(self.idx(0, 0, 0), self.idx(dz, 0, 0), dz - 1)

    def out_y(self, dz):
        return self.copy(self.idx(-dz, 0, 0), self.idx(0, 1, 0), self.outer - 1 + dz)

    def out_c(self, dz, dy):
        slot = 2 * self.outer - 1 + 2 * dz + dy
        return self.copy(self.idx(-dz, dy, 0), self.idx(0, 0, 1), slot)

    def start(self):
        for dz in range(1, self.outer):
            self.out_z(dz).start()
        self.out_y(0).start()
        self.out_c(0, 0).start()

    def arrive(self, dz, dy):
        if dy == 1:
            self.copy(self.idx(-dz, 1, 0), self.idx(0, 1, 0), self.outer - 1 + dz).wait_recv()
            self.out_c(dz, 1).start()
        elif dz > 0:
            self.copy(self.idx(-dz, 0, 0), self.idx(-dz, 0, 0), dz - 1).wait_recv()
            self.out_y(dz).start()
            self.out_c(dz, 0).start()

    def ready(self, dz, dy):
        slot = 2 * self.outer - 1 + 2 * dz + dy
        self.copy(self.idx(-dz, dy, 1), self.idx(0, 0, 1), slot).wait_recv()

    def sent(self):
        for dz in range(1, self.outer):
            self.out_z(dz).wait_send()
        for dz in range(self.outer):
            self.out_y(dz).wait_send()
            for dy in range(2):
                self.out_c(dz, dy).wait_send()

    def events(self):
        return [(dz, dy) for dz in range(self.outer) for dy in range(2)]

    def finish(self):
        for event in self.events():
            self.arrive(*event)
        for event in self.events():
            self.ready(*event)


def exchange(buf, send, recv, me, n, shift):
    return pltpu.make_async_remote_copy(
        src_ref=buf.at[me],
        dst_ref=buf.at[me],
        send_sem=send.at[shift - 1],
        recv_sem=recv.at[shift - 1],
        device_id={"tp": lax.rem(me + shift, n)},
        device_id_type=pl.DeviceIdType.MESH,
    )


def received(buf, send, recv, me, n, shift):
    block = lax.rem(me - shift + n, n)
    return pltpu.make_async_remote_copy(
        src_ref=buf.at[block],
        dst_ref=buf.at[block],
        send_sem=send.at[shift - 1],
        recv_sem=recv.at[shift - 1],
        device_id={"tp": block},
        device_id_type=pl.DeviceIdType.MESH,
    )


def kernel(
    n,
    tokens, carried, proj_in, proj_gate, proj_out, norm_params,
    lam_re, lam_im, log_step, in_c, out_c, skip,
    stream_out, new_carried,
    xg, pg, g1, g2, nb, sb, win, wgate, wcat, pown, states, fresh, acc, decay, bbar, outb,
    gsend, grecv, nsend, nrecv, ssend, srecv, lsem,
):
    me = lax.axis_index("tp")
    outer = n // 4
    place = (me // 4, lax.rem(me // 2, 2), lax.rem(me, 2))
    layers, groups, state = lam_re.shape
    rows, width = tokens.shape
    ssm = proj_out.shape[1]
    own = proj_in.shape[2]
    ch = own // groups

    loads = [
        pltpu.make_async_copy(tokens, xg.at[me], lsem.at[0]),
        pltpu.make_async_copy(proj_out.at[0], pg.at[me], lsem.at[1]),
        pltpu.make_async_copy(norm_params, nb.at[me], lsem.at[2]),
        pltpu.make_async_copy(proj_in, win, lsem.at[3]),
        pltpu.make_async_copy(proj_gate, wgate, lsem.at[4]),
        pltpu.make_async_copy(carried, states, lsem.at[5]),
        pltpu.make_async_copy(proj_out.at[1], pown, lsem.at[6]),
    ]
    for load in loads:
        load.start()
    barrier = pltpu.get_barrier_semaphore()
    for shift in range(1, n):
        pl.semaphore_signal(
            barrier, inc=1, device_id={"tp": lax.rem(me + shift, n)}, device_id_type=pl.DeviceIdType.MESH
        )
    pl.semaphore_wait(barrier, n - 1)

    ga = Gather(xg, gsend.at[0], grecv.at[0], place, outer)
    gp = Gather(pg, gsend.at[1], grecv.at[1], place, outer)
    gg = [Gather(g1, gsend.at[2], grecv.at[2], place, outer), Gather(g2, gsend.at[3], grecv.at[3], place, outer)]
    loads[0].wait()
    ga.start()
    loads[2].wait()
    for shift in range(1, n):
        exchange(nb, nsend, nrecv, me, n, shift).start()
    loads[1].wait()
    gp.start()

    loads[3].wait()
    loads[4].wait()
    for l in range(layers):
        wcat[l] = jnp.concatenate([win[l], wgate[l]], axis=1)
    for l in range(layers):
        for g in range(groups):
            lr = lam_re[l, g : g + 1, :]
            li = lam_im[l, g : g + 1, :]
            step_len = jnp.exp(log_step[l : l + 1, g : g + 1])
            modulus = jnp.exp(lr * step_len)
            d_re = modulus * jnp.cos(li * step_len)
            d_im = modulus * jnp.sin(li * step_len)
            den = lr * lr + li * li
            shifted = d_re - 1.0
            k_re = column((shifted * lr + d_im * li) / den)
            k_im = column((d_im * lr - shifted * li) / den)
            decay[l, g, 0] = column(d_re)
            decay[l, g, 1] = column(d_im)
            bbar[l, g, :state] = k_re * in_c[l, 0, g] - k_im * in_c[l, 1, g]
            bbar[l, g, state:] = k_re * in_c[l, 1, g] + k_im * in_c[l, 0, g]

    def pair_dot(dz, dy, first):
        j = ga.idx(-dz, dy, 0) // 2
        lhs = jnp.concatenate([xg[2 * j], xg[2 * j + 1]], axis=1)
        rhs = wcat[0, pl.ds(pl.multiple_of(j * (2 * width), 2 * width), 2 * width), :]
        part = jnp.dot(lhs, rhs, preferred_element_type=F32)
        if first:
            acc[...] = part
        else:
            acc[...] += part

    events = ga.events()
    for i, event in enumerate(events):
        ga.arrive(*event)
        if i > 0:
            ga.ready(*events[i - 1])
            pair_dot(*events[i - 1], i == 1)
    ga.ready(*events[-1])
    pair_dot(*events[-1], False)

    def mixer(l, gbuf, between):
        pre_t = acc[...].astype(BF16).astype(F32).T
        skip_col = column(skip[l : l + 1, :])
        parts = []
        for g in range(groups):
            drive = pre_t[g * ch : (g + 1) * ch]
            push = jnp.dot(bbar[l, g], drive, precision=HIGHEST, preferred_element_type=F32)
            old_re, old_im = states[l, 0, g], states[l, 1, g]
            d_re, d_im = decay[l, g, 0], decay[l, g, 1]
            new_re = d_re * old_re - d_im * old_im + push[:state]
            new_im = d_re * old_im + d_im * old_re + push[state:]
            fresh[l, 0, g] = new_re
            fresh[l, 1, g] = new_im
            parts.append(
                jnp.dot(out_c[l, 0, g], new_re, precision=HIGHEST, preferred_element_type=F32)
                - jnp.dot(out_c[l, 1, g], new_im, precision=HIGHEST, preferred_element_type=F32)
                + skip_col[g * ch : (g + 1) * ch] * drive
            )
            between(g)
        y = jnp.concatenate(parts, axis=0) if groups > 1 else parts[0]
        gbuf[me] = (jax.nn.gelu(y) * jax.nn.sigmoid(pre_t[own:])).astype(BF16)

    p_events = gp.events()
    for event in p_events[: len(p_events) // 4]:
        gp.arrive(*event)
    loads[5].wait()

    def p_step(g):
        share = len(p_events) // 4
        if g == 0:
            for event in p_events[share : 2 * share]:
                gp.arrive(*event)

    mixer(0, g1, p_step)
    gg[0].start()
    stores = [pltpu.make_async_copy(fresh.at[0], new_carried.at[0], lsem.at[7])]
    stores[0].start()
    for event in p_events[len(p_events) // 4 * 2 :]:
        gp.arrive(*event)
    for event in p_events:
        gp.ready(*event)
    gg[0].finish()
    for shift in range(1, n):
        received(nb, nsend, nrecv, me, n, shift).wait_recv()
    ga.sent()

    chunk = min(rows, 128)

    def row_chunk(r, carry):
        at = pl.ds(pl.multiple_of(r * chunk, chunk), chunk)
        gated = g1[:, :, at].reshape(ssm, chunk).astype(F32).T.astype(BF16)
        total = jnp.zeros((chunk, 1), F32)
        square = jnp.zeros((chunk, 1), F32)
        wide = []
        for j in range(n // 2):
            weights = jnp.concatenate([pg[2 * j], pg[2 * j + 1]], axis=1)
            mixed = jnp.dot(gated, weights, preferred_element_type=F32)
            old = jnp.concatenate([xg[2 * j, at, :], xg[2 * j + 1, at, :]], axis=1)
            summed = (RESIDUAL_SCALE * old.astype(F32) + mixed).astype(BF16)
            s = summed.astype(F32)
            total += jnp.sum(s, axis=1, keepdims=True)
            square += jnp.sum(s * s, axis=1, keepdims=True)
            wide.append(summed)
        mean = total / (n * width)
        var = square / (n * width) - mean * mean
        scale = lax.rsqrt(var + NORM_EPS)
        pre = jnp.zeros((chunk, 2 * own), F32)
        for j in range(n // 2):
            par = jnp.concatenate([nb[2 * j, 0], nb[2 * j + 1, 0]], axis=1).astype(F32)
            out = ((wide[j].astype(F32) - mean) * scale * par[0:1] + par[1:2]).astype(BF16)
            xg[2 * j, at, :] = out[:, :width]
            xg[2 * j + 1, at, :] = out[:, width:]
            pre += jnp.dot(out, wcat[1, 2 * j * width : 2 * (j + 1) * width, :], preferred_element_type=F32)
        acc[at, :] = pre
        return carry

    lax.fori_loop(0, rows // chunk, row_chunk, 0)

    mixer(1, g2, lambda g: None)
    gg[1].start()
    stores.append(pltpu.make_async_copy(fresh.at[1], new_carried.at[1], lsem.at[8]))
    stores[1].start()
    residual_t = RESIDUAL_SCALE * xg[me].astype(F32).T
    gain = column(nb[me, 1].astype(F32)[0:1])
    bias = column(nb[me, 1].astype(F32)[1:2])
    loads[6].wait()
    weights_t = pown[...].astype(F32).T.astype(BF16)
    gg[1].finish()
    mixed_t = jnp.dot(weights_t, g2[...].reshape(ssm, rows), preferred_element_type=F32)
    s = (residual_t + mixed_t).astype(BF16).astype(F32)
    sb[me] = jnp.concatenate([jnp.sum(s, axis=0, keepdims=True), jnp.sum(s * s, axis=0, keepdims=True)], axis=0)
    for shift in range(1, n):
        exchange(sb, ssend, srecv, me, n, shift).start()
    for shift in range(1, n):
        received(sb, ssend, srecv, me, n, shift).wait_recv()
    sums = jnp.sum(sb[...], axis=0) / (n * width)
    mean = sums[0:1]
    scale = lax.rsqrt(sums[1:2] - mean * mean + NORM_EPS)
    outb[...] = ((s - mean) * scale * gain + bias).T.astype(BF16)
    last = pltpu.make_async_copy(outb, stream_out, lsem.at[9])
    last.start()
    for gather in (gp, gg[0], gg[1]):
        gather.sent()
    for shift in range(1, n):
        exchange(nb, nsend, nrecv, me, n, shift).wait_send()
        exchange(sb, ssend, srecv, me, n, shift).wait_send()
    for store in stores:
        store.wait()
    last.wait()


def per_device(n, *args):
    tokens, carried, proj_in, _, proj_out, norm_params, lam_re = args[:7]
    rows, width = tokens.shape
    layers, groups, state = lam_re.shape
    ssm, own = proj_out.shape[1], proj_in.shape[2]
    any_space = pl.BlockSpec(memory_space=pl.ANY)
    vmem = pl.BlockSpec(memory_space=pltpu.VMEM)
    slots = n - 1
    dma = pltpu.SemaphoreType.DMA
    return pl.pallas_call(
        functools.partial(kernel, n),
        out_shape=(
            jax.ShapeDtypeStruct(tokens.shape, tokens.dtype),
            jax.ShapeDtypeStruct(carried.shape, carried.dtype),
        ),
        in_specs=[any_space] * 6 + [vmem] * 6,
        out_specs=(any_space, any_space),
        scratch_shapes=[
            pltpu.VMEM((n, rows, width), BF16),
            pltpu.VMEM((n, ssm, width), BF16),
            pltpu.VMEM((n, own, rows), BF16),
            pltpu.VMEM((n, own, rows), BF16),
            pltpu.VMEM((n,) + norm_params.shape, BF16),
            pltpu.VMEM((n, 2, rows), F32),
            pltpu.VMEM(proj_in.shape, BF16),
            pltpu.VMEM(proj_in.shape, BF16),
            pltpu.VMEM(proj_in.shape[:2] + (2 * own,), BF16),
            pltpu.VMEM(proj_out.shape[1:], BF16),
            pltpu.VMEM(carried.shape, F32),
            pltpu.VMEM(carried.shape, F32),
            pltpu.VMEM((rows, 2 * own), F32),
            pltpu.VMEM((layers, groups, 2, state, 1), F32),
            pltpu.VMEM((layers, groups, 2 * state, own // groups), F32),
            pltpu.VMEM((rows, width), BF16),
            dma((4, slots)),
            dma((4, slots)),
            dma((n - 1,)),
            dma((n - 1,)),
            dma((n - 1,)),
            dma((n - 1,)),
            dma((10,)),
        ],
        compiler_params=pltpu.CompilerParams(
            collective_id=0, has_side_effects=True, vmem_limit_bytes=60 * 1024 * 1024
        ),
    )(*args)


def solution(mesh):
    return jax.shard_map(
        functools.partial(per_device, mesh.shape["tp"]),
        mesh=mesh,
        in_specs=(
            P("grp", "tp"),
            P(None, None, "tp", None, "grp"),
            P(None, None, "tp"),
            P(None, None, "tp"),
            P(None, None, "tp"),
            P(None, None, "tp"),
            P(None, "tp", None),
            P(None, "tp", None),
            P(None, "tp"),
            P(None, None, "tp", None, None),
            P(None, None, "tp", None, None),
            P(None, "tp"),
        ),
        out_specs=(P("grp", "tp"), P(None, None, "tp", None, "grp")),
        check_vma=False,
    )
```

time: 224 us -> 122 us (0.54)
  waiting for transfers between devices: 151 us -> 0 us
  Pallas kernels: 0 us -> 110 us
  matrix products: 26.5 us -> 0 us
  blocking collectives: 19 us -> 0 us
  between operations: 14 us -> 0.64 us
  other arithmetic: 7.94 us -> 0 us
  local copies, waits for them, and re-layouts: 5.24 us -> 11.1 us
    all_gather x4 -> x0, waiting for transfers between devices: 150 us -> none  [the longest x2 74 us: per_device(): gated_all = lax.all_gather(gated, 'tp', axis=1, tiled=True)]
    pallas_call x0 -> x1, Pallas kernels: none -> 110 us  [per_device(): pl.pallas_call(functools.partial(kernel, n), out_shape=(jax.ShapeDtypeStr...]
    dot_general x14 -> x0, matrix products: 26.5 us -> none  [the longest x2 13.3 us: per_device(): jnp.dot(gated_all, out_whole[layer_idx], preferred_element_type=jnp.float32)]
    all_gather x1 -> x0, blocking collectives: 19 us -> none  [per_device(): lax.all_gather(norm_params, 'tp', axis=2, tiled=True)]
    unnamed x26 -> x5, local copies, waits for them, and re-layouts: 1.81 us -> 11.1 us
    div x5 -> x0, other arithmetic: 3.41 us -> none  [the longest x2 2.69 us: discretize(): coef_re = (shifted * lam_re + decay_im * lam_im) / denominator]
    convert_element_type x3 -> x0, other arithmetic: 2.93 us -> none  [the longest x2 2.91 us: norm_whole(): (scaled * params[0].astype(jnp.float32) + params[1].astype(jnp.float32))....]
  transfers between devices with their start and end apart: 4 -> 0, of which waited for: 4 -> 0; matrix products, arithmetic and copies ran while one was open for 7% -> 0% of each run, Pallas kernels for 0% -> 0%
where the time goes in v1:
time: 122 us
  Pallas kernels  110 us (90%)
  local copies, waits for them, and re-layouts  11.1 us (9%)
    pallas_call x1, Pallas kernels, per_device(): pl.pallas_call(functools.partial(kernel, n), out_shape=(jax.ShapeDtypeStr...  110 us
    unnamed x5, local copies, waits for them, and re-layouts  11.1 us

profile of v1, /device:TPU:0, one launch (start us, length us, event | category | flops | bytes accessed | tf_op | source)
XLA Modules:
  0.0 121.9 jit_solution(9975130300787672587)
XLA Ops:
  0.6 1.7 %copy.16.in_c = f32[2,2,2,64,16]{4,3,2,1,0:T(8,128)} copy(f32[2,2,2,64,16]{3,4,2,1,0:T(8,128)} %param.21) | data formatting | bytes 65536 | tf_op args[9]
  2.3 2.3 %copy.14.proj_in = bf16[2,2048,32]{2,1,0:T(8,128)(2,1)} copy(bf16[2,2048,32]{1,2,0:T(8,128)(2,1)} %param.14) | data formatting | bytes 524288 | tf_op args[2]
  4.6 2.3 %copy.15.proj_gate = bf16[2,2048,32]{2,1,0:T(8,128)(2,1)} copy(bf16[2,2048,32]{1,2,0:T(8,128)(2,1)} %param.15) | data formatting | bytes 524288 | tf_op args[3]
  6.9 110.2 %shard_map.131 = (bf16[1024,128]{1,0:T(8,128)(2,1)}, f32[2,2,2,64,1024]{4,3,2,1,0:T(8,128)}) custom-call(bf16[1024,128]{1,0:T(8,128)(2,1)} %tokens.1, f32[2,2,2,64,1024]{4,3,2,1,0:T(8,128)} %carried.1, bf16[2,2048,32]{2,1,0:T(8,128)(2,1)} %copy.14.proj_in, bf16[2,2048,32]{2,1,0:T(8,128)(2,1)} %copy.15.proj_gate, bf16[2,512,128]{2,1,0:T(8,128)(2,1)} %proj_out.1, ...), custom_call_target="tpu_custom_call" | custom-call | tf_op jit(solution)/shard_map/pallas_call | solution.py:320
  117.1 1.7 %copy.19 = bf16[1024,128]{1,0:T(8,128)(2,1)} copy(bf16[1024,128]{1,0:T(8,128)(2,1)} %get-tuple-element.4) | data formatting | bytes 524288
  118.8 3.2 %copy.20 = f32[2,2,2,64,1024]{4,3,2,1,0:T(8,128)} copy(f32[2,2,2,64,1024]{4,3,2,1,0:T(8,128)} %get-tuple-element.5) | data formatting | bytes 4194304

commit v2 on v1

--- a/solution.py
+++ b/solution.py
@@ -12,6 +12,7 @@
 HIGHEST = lax.Precision.HIGHEST
 F32 = jnp.float32
 BF16 = jnp.bfloat16
+VMEM_BYTES = 67043328
 
 
 def column(row):
@@ -21,7 +22,8 @@
 
 
 class Gather:
-    def __init__(self, buf, send, recv, place, outer):
+    def __init__(self, buf, send, recv, place, outer, part=None):
+        self.part = part
         self.buf, self.send, self.recv, self.outer = buf, send, recv, outer
         self.z, self.y, self.c = place
 
@@ -32,9 +34,10 @@
         return (z * 2 + y) * 2 + c
 
     def copy(self, block, target, slot):
+        ref = self.buf.at[block] if self.part is None else self.buf.at[block, self.part]
         return pltpu.make_async_remote_copy(
-            src_ref=self.buf.at[block],
-            dst_ref=self.buf.at[block],
+            src_ref=ref,
+            dst_ref=ref,
             send_sem=self.send.at[slot],
             recv_sem=self.recv.at[slot],
             device_id={"tp": target},
@@ -52,9 +55,9 @@
         return self.copy(self.idx(-dz, dy, 0), self.idx(0, 0, 1), slot)
 
     def start(self):
+        self.out_y(0).start()
         for dz in range(1, self.outer):
             self.out_z(dz).start()
-        self.out_y(0).start()
         self.out_c(0, 0).start()
 
     def arrive(self, dz, dy):
@@ -114,9 +117,10 @@
 def kernel(
     n,
     tokens, carried, proj_in, proj_gate, proj_out, norm_params,
-    lam_re, lam_im, log_step, in_c, out_c, skip,
+    lam_re_h, lam_im_h, log_step_h, in_c_h, out_c_h, skip_h,
     stream_out, new_carried,
     xg, pg, g1, g2, nb, sb, win, wgate, wcat, pown, states, fresh, acc, decay, bbar, outb,
+    lam_re, lam_im, log_step, in_c, out_c, skip,
     gsend, grecv, nsend, nrecv, ssend, srecv, lsem,
 ):
     me = lax.axis_index("tp")
@@ -125,7 +129,7 @@
     layers, groups, state = lam_re.shape
     rows, width = tokens.shape
     ssm = proj_out.shape[1]
-    own = proj_in.shape[2]
+    own = proj_in.shape[1]
     ch = own // groups
 
     loads = [
@@ -137,7 +141,9 @@
         pltpu.make_async_copy(carried, states, lsem.at[5]),
         pltpu.make_async_copy(proj_out.at[1], pown, lsem.at[6]),
     ]
-    for load in loads:
+    small = [(lam_re_h, lam_re), (lam_im_h, lam_im), (log_step_h, log_step), (in_c_h, in_c), (out_c_h, out_c), (skip_h, skip)]
+    params = [pltpu.make_async_copy(a, b, lsem.at[10 + i]) for i, (a, b) in enumerate(small)]
+    for load in loads[:5] + params + loads[5:]:
         load.start()
     barrier = pltpu.get_barrier_semaphore()
     for shift in range(1, n):
@@ -146,11 +152,16 @@
         )
     pl.semaphore_wait(barrier, n - 1)
 
-    ga = Gather(xg, gsend.at[0], grecv.at[0], place, outer)
+    half = rows // 2
+    halves = [
+        Gather(xg, gsend.at[k], grecv.at[k], place, outer, pl.ds(part * half, half))
+        for part, k in enumerate((0, 4))
+    ]
     gp = Gather(pg, gsend.at[1], grecv.at[1], place, outer)
     gg = [Gather(g1, gsend.at[2], grecv.at[2], place, outer), Gather(g2, gsend.at[3], grecv.at[3], place, outer)]
     loads[0].wait()
-    ga.start()
+    for ga in halves:
+        ga.start()
     loads[2].wait()
     for shift in range(1, n):
         exchange(nb, nsend, nrecv, me, n, shift).start()
@@ -159,8 +170,10 @@
 
     loads[3].wait()
     loads[4].wait()
+    for load in params:
+        load.wait()
     for l in range(layers):
-        wcat[l] = jnp.concatenate([win[l], wgate[l]], axis=1)
+        wcat[l] = jnp.concatenate([win[l], wgate[l]], axis=0).astype(F32).T.astype(BF16)
     for l in range(layers):
         for g in range(groups):
             lr = lam_re[l, g : g + 1, :]
@@ -171,31 +184,33 @@
             d_im = modulus * jnp.sin(li * step_len)
             den = lr * lr + li * li
             shifted = d_re - 1.0
-            k_re = column((shifted * lr + d_im * li) / den)
-            k_im = column((d_im * lr - shifted * li) / den)
+            k_re = (shifted * lr + d_im * li) / den
+            k_im = (d_im * lr - shifted * li) / den
             decay[l, g, 0] = column(d_re)
             decay[l, g, 1] = column(d_im)
-            bbar[l, g, :state] = k_re * in_c[l, 0, g] - k_im * in_c[l, 1, g]
-            bbar[l, g, state:] = k_re * in_c[l, 1, g] + k_im * in_c[l, 0, g]
-
-    def pair_dot(dz, dy, first):
+            bbar[l, g, :state] = (k_re * in_c[l, 0, g] - k_im * in_c[l, 1, g]).T
+            bbar[l, g, state:] = (k_re * in_c[l, 1, g] + k_im * in_c[l, 0, g]).T
+
+    def pair_dot(ga, dz, dy, first):
         j = ga.idx(-dz, dy, 0) // 2
-        lhs = jnp.concatenate([xg[2 * j], xg[2 * j + 1]], axis=1)
+        lhs = jnp.concatenate([xg[2 * j, ga.part, :], xg[2 * j + 1, ga.part, :]], axis=1)
         rhs = wcat[0, pl.ds(pl.multiple_of(j * (2 * width), 2 * width), 2 * width), :]
         part = jnp.dot(lhs, rhs, preferred_element_type=F32)
         if first:
-            acc[...] = part
+            acc[ga.part, :] = part
         else:
-            acc[...] += part
-
-    events = ga.events()
-    for i, event in enumerate(events):
-        ga.arrive(*event)
-        if i > 0:
-            ga.ready(*events[i - 1])
-            pair_dot(*events[i - 1], i == 1)
-    ga.ready(*events[-1])
-    pair_dot(*events[-1], False)
+            acc[ga.part, :] += part
+
+    due = None
+    for ga in halves:
+        for i, event in enumerate(ga.events()):
+            ga.arrive(*event)
+            if due is not None:
+                due[0].ready(*due[1])
+                pair_dot(due[0], *due[1], due[2])
+            due = (ga, event, i == 0)
+    due[0].ready(*due[1])
+    pair_dot(due[0], *due[1], due[2])
 
     def mixer(l, gbuf, between):
         pre_t = acc[...].astype(BF16).astype(F32).T
@@ -241,7 +256,8 @@
     gg[0].finish()
     for shift in range(1, n):
         received(nb, nsend, nrecv, me, n, shift).wait_recv()
-    ga.sent()
+    for ga in halves:
+        ga.sent()
 
     chunk = min(rows, 128)
 
@@ -308,22 +324,33 @@
     last.wait()
 
 
+def deliver(stream, fresh, stream_out, new_carried, sem):
+    copies = [pltpu.make_async_copy(stream, stream_out, sem.at[0]), pltpu.make_async_copy(fresh, new_carried, sem.at[1])]
+    for copy in copies:
+        copy.start()
+    for copy in copies:
+        copy.wait()
+
+
 def per_device(n, *args):
+    args = list(args)
+    for i in (2, 3, 9):
+        args[i] = jnp.swapaxes(args[i], -1, -2)
     tokens, carried, proj_in, _, proj_out, norm_params, lam_re = args[:7]
     rows, width = tokens.shape
     layers, groups, state = lam_re.shape
-    ssm, own = proj_out.shape[1], proj_in.shape[2]
+    ssm, own = proj_out.shape[1], proj_in.shape[1]
     any_space = pl.BlockSpec(memory_space=pl.ANY)
-    vmem = pl.BlockSpec(memory_space=pltpu.VMEM)
     slots = n - 1
+    delivered = carried.size * 4 + rows * max(width, 128) * 2
     dma = pltpu.SemaphoreType.DMA
-    return pl.pallas_call(
+    stream, fresh = pl.pallas_call(
         functools.partial(kernel, n),
         out_shape=(
-            jax.ShapeDtypeStruct(tokens.shape, tokens.dtype),
-            jax.ShapeDtypeStruct(carried.shape, carried.dtype),
+            pltpu.VMEM(tokens.shape, tokens.dtype),
+            pltpu.VMEM(carried.shape, carried.dtype),
         ),
-        in_specs=[any_space] * 6 + [vmem] * 6,
+        in_specs=[pl.BlockSpec(memory_space=pltpu.HBM)] * len(args),
         out_specs=(any_space, any_space),
         scratch_shapes=[
             pltpu.VMEM((n, rows, width), BF16),
@@ -334,7 +361,7 @@
             pltpu.VMEM((n, 2, rows), F32),
             pltpu.VMEM(proj_in.shape, BF16),
             pltpu.VMEM(proj_in.shape, BF16),
-            pltpu.VMEM(proj_in.shape[:2] + (2 * own,), BF16),
+            pltpu.VMEM((layers, n * width, 2 * own), BF16),
             pltpu.VMEM(proj_out.shape[1:], BF16),
             pltpu.VMEM(carried.shape, F32),
             pltpu.VMEM(carried.shape, F32),
@@ -342,18 +369,30 @@
             pltpu.VMEM((layers, groups, 2, state, 1), F32),
             pltpu.VMEM((layers, groups, 2 * state, own // groups), F32),
             pltpu.VMEM((rows, width), BF16),
-            dma((4, slots)),
-            dma((4, slots)),
+            *[pltpu.VMEM(a.shape, a.dtype) for a in args[6:]],
+            dma((5, slots)),
+            dma((5, slots)),
             dma((n - 1,)),
             dma((n - 1,)),
             dma((n - 1,)),
             dma((n - 1,)),
-            dma((10,)),
+            dma((10 + len(args) - 6,)),
         ],
         compiler_params=pltpu.CompilerParams(
-            collective_id=0, has_side_effects=True, vmem_limit_bytes=60 * 1024 * 1024
+            collective_id=0, has_side_effects=True, vmem_limit_bytes=VMEM_BYTES - delivered - (1 << 18)
         ),
     )(*args)
+    return pl.pallas_call(
+        deliver,
+        out_shape=(
+            jax.ShapeDtypeStruct(tokens.shape, tokens.dtype),
+            jax.ShapeDtypeStruct(carried.shape, carried.dtype),
+        ),
+        in_specs=[any_space] * 2,
+        out_specs=(any_space, any_space),
+        scratch_shapes=[dma((2,))],
+        compiler_params=pltpu.CompilerParams(vmem_limit_bytes=1024 * 1024),
+    )(stream, fresh)
 
 
 def solution(mesh):

time: 122 us -> 108 us (0.89)
  local copies, waits for them, and re-layouts: 11.1 us -> 0 us
  Pallas kernels: 110 us -> 108 us
    unnamed x5 -> x0, local copies, waits for them, and re-layouts: 11.1 us -> none
    pallas_call x1 -> x2, Pallas kernels: 110 us -> 108 us  [the longest x1 106 us: per_device(): pl.pallas_call(functools.partial(kernel, n), out_shape=(pltpu.VMEM(tokens...]
where the time goes in v2:
time: 108 us
  Pallas kernels  108 us (100%)
    pallas_call x1, Pallas kernels, per_device(): pl.pallas_call(functools.partial(kernel, n), out_shape=(pltpu.VMEM(tokens...  106 us

profile of v2, /device:TPU:0, one launch (start us, length us, event | category | flops | bytes accessed | tf_op | source)
XLA Modules:
  0.0 108.2 jit_solution(11801730025245158119)
XLA Ops:
  0.6 106.1 %shard_map.131 = (bf16[1024,128]{1,0:T(8,128)(2,1)S(1)}, f32[2,2,2,64,1024]{4,3,2,1,0:T(8,128)S(1)}) custom-call(bf16[1024,128]{1,0:T(8,128)(2,1)} %tokens.1, f32[2,2,2,64,1024]{4,3,2,1,0:T(8,128)} %carried.1, bf16[2,32,2048]{2,1,0:T(8,128)(2,1)} %bitcast.3, bf16[2,32,2048]{2,1,0:T(8,128)(2,1)} %bitcast.4, bf16[2,512,128]{2,1,0:T(8,128)(2,1)} %proj_out.1, ...), custom_call_target="tpu_custom_call" | custom-call | tf_op jit(solution)/shard_map/pallas_call | solution.py:347
  106.8 1.4 %shard_map.132 = (bf16[1024,128]{1,0:T(8,128)(2,1)}, f32[2,2,2,64,1024]{4,3,2,1,0:T(8,128)}) custom-call(bf16[1024,128]{1,0:T(8,128)(2,1)S(1)} %get-tuple-element.4.stream, f32[2,2,2,64,1024]{4,3,2,1,0:T(8,128)S(1)} %get-tuple-element.5.fresh), custom_call_target="tpu_custom_call" | custom-call | tf_op jit(solution)/shard_map/pallas_call | solution.py:385

commit v3 on v2

--- a/solution.py
+++ b/solution.py
@@ -158,7 +158,8 @@
         for part, k in enumerate((0, 4))
     ]
     gp = Gather(pg, gsend.at[1], grecv.at[1], place, outer)
-    gg = [Gather(g1, gsend.at[2], grecv.at[2], place, outer), Gather(g2, gsend.at[3], grecv.at[3], place, outer)]
+    g_in = [Gather(g1.at[h], gsend.at[2 + h], grecv.at[2 + h], place, outer) for h in range(2)]
+    g_out = [Gather(g2.at[h], gsend.at[5 + h], grecv.at[5 + h], place, outer) for h in range(2)]
     loads[0].wait()
     for ga in halves:
         ga.start()
@@ -201,69 +202,69 @@
         else:
             acc[ga.part, :] += part
 
-    due = None
-    for ga in halves:
+    def token_half(ga):
+        due = None
         for i, event in enumerate(ga.events()):
             ga.arrive(*event)
             if due is not None:
-                due[0].ready(*due[1])
-                pair_dot(due[0], *due[1], due[2])
-            due = (ga, event, i == 0)
-    due[0].ready(*due[1])
-    pair_dot(due[0], *due[1], due[2])
-
-    def mixer(l, gbuf, between):
-        pre_t = acc[...].astype(BF16).astype(F32).T
+                ga.ready(*due)
+                pair_dot(ga, *due, i == 1)
+            due = event
+        ga.ready(*due)
+        pair_dot(ga, *due, False)
+
+    def mixer(l, gbuf, h):
+        at = pl.ds(h * half, half)
+        pre_t = acc[at, :].astype(BF16).astype(F32).T
         skip_col = column(skip[l : l + 1, :])
         parts = []
         for g in range(groups):
             drive = pre_t[g * ch : (g + 1) * ch]
             push = jnp.dot(bbar[l, g], drive, precision=HIGHEST, preferred_element_type=F32)
-            old_re, old_im = states[l, 0, g], states[l, 1, g]
+            old_re, old_im = states[l, 0, g, :, at], states[l, 1, g, :, at]
             d_re, d_im = decay[l, g, 0], decay[l, g, 1]
             new_re = d_re * old_re - d_im * old_im + push[:state]
             new_im = d_re * old_im + d_im * old_re + push[state:]
-            fresh[l, 0, g] = new_re
-            fresh[l, 1, g] = new_im
+            fresh[l, 0, g, :, at] = new_re
+            fresh[l, 1, g, :, at] = new_im
             parts.append(
                 jnp.dot(out_c[l, 0, g], new_re, precision=HIGHEST, preferred_element_type=F32)
                 - jnp.dot(out_c[l, 1, g], new_im, precision=HIGHEST, preferred_element_type=F32)
                 + skip_col[g * ch : (g + 1) * ch] * drive
             )
-            between(g)
         y = jnp.concatenate(parts, axis=0) if groups > 1 else parts[0]
-        gbuf[me] = (jax.nn.gelu(y) * jax.nn.sigmoid(pre_t[own:])).astype(BF16)
-
+        gbuf[h, me] = (jax.nn.gelu(y) * jax.nn.sigmoid(pre_t[own:])).astype(BF16)
+
+    token_half(halves[0])
+    loads[5].wait()
+    mixer(0, g1, 0)
+    g_in[0].start()
+    token_half(halves[1])
     p_events = gp.events()
-    for event in p_events[: len(p_events) // 4]:
+    for event in p_events[: len(p_events) // 2]:
         gp.arrive(*event)
-    loads[5].wait()
-
-    def p_step(g):
-        share = len(p_events) // 4
-        if g == 0:
-            for event in p_events[share : 2 * share]:
-                gp.arrive(*event)
-
-    mixer(0, g1, p_step)
-    gg[0].start()
+    mixer(0, g1, 1)
+    g_in[1].start()
     stores = [pltpu.make_async_copy(fresh.at[0], new_carried.at[0], lsem.at[7])]
     stores[0].start()
-    for event in p_events[len(p_events) // 4 * 2 :]:
+    for event in p_events[len(p_events) // 2 :]:
         gp.arrive(*event)
+    for event in g_in[0].events():
+        g_in[0].arrive(*event)
     for event in p_events:
         gp.ready(*event)
-    gg[0].finish()
+    for event in g_in[0].events():
+        g_in[0].ready(*event)
     for shift in range(1, n):
         received(nb, nsend, nrecv, me, n, shift).wait_recv()
     for ga in halves:
         ga.sent()
 
-    chunk = min(rows, 128)
-
-    def row_chunk(r, carry):
-        at = pl.ds(pl.multiple_of(r * chunk, chunk), chunk)
-        gated = g1[:, :, at].reshape(ssm, chunk).astype(F32).T.astype(BF16)
+    chunk = min(half, 128)
+
+    def row_chunk(h, r, carry):
+        at = pl.ds(pl.multiple_of(h * half + r * chunk, chunk), chunk)
+        gated = g1[h, :, :, pl.ds(pl.multiple_of(r * chunk, chunk), chunk)].reshape(ssm, chunk).astype(F32).T.astype(BF16)
         total = jnp.zeros((chunk, 1), F32)
         square = jnp.zeros((chunk, 1), F32)
         wide = []
@@ -289,10 +290,13 @@
         acc[at, :] = pre
         return carry
 
-    lax.fori_loop(0, rows // chunk, row_chunk, 0)
-
-    mixer(1, g2, lambda g: None)
-    gg[1].start()
+    lax.fori_loop(0, half // chunk, functools.partial(row_chunk, 0), 0)
+    mixer(1, g2, 0)
+    g_out[0].start()
+    g_in[1].finish()
+    lax.fori_loop(0, half // chunk, functools.partial(row_chunk, 1), 0)
+    mixer(1, g2, 1)
+    g_out[1].start()
     stores.append(pltpu.make_async_copy(fresh.at[1], new_carried.at[1], lsem.at[8]))
     stores[1].start()
     residual_t = RESIDUAL_SCALE * xg[me].astype(F32).T
@@ -300,9 +304,12 @@
     bias = column(nb[me, 1].astype(F32)[1:2])
     loads[6].wait()
     weights_t = pown[...].astype(F32).T.astype(BF16)
-    gg[1].finish()
-    mixed_t = jnp.dot(weights_t, g2[...].reshape(ssm, rows), preferred_element_type=F32)
-    s = (residual_t + mixed_t).astype(BF16).astype(F32)
+    sums = []
+    for h in range(2):
+        g_out[h].finish()
+        mixed_t = jnp.dot(weights_t, g2[h].reshape(ssm, half), preferred_element_type=F32)
+        sums.append((residual_t[:, h * half : (h + 1) * half] + mixed_t).astype(BF16).astype(F32))
+    s = jnp.concatenate(sums, axis=1)
     sb[me] = jnp.concatenate([jnp.sum(s, axis=0, keepdims=True), jnp.sum(s * s, axis=0, keepdims=True)], axis=0)
     for shift in range(1, n):
         exchange(sb, ssend, srecv, me, n, shift).start()
@@ -314,7 +321,7 @@
     outb[...] = ((s - mean) * scale * gain + bias).T.astype(BF16)
     last = pltpu.make_async_copy(outb, stream_out, lsem.at[9])
     last.start()
-    for gather in (gp, gg[0], gg[1]):
+    for gather in (gp, *g_in, *g_out):
         gather.sent()
     for shift in range(1, n):
         exchange(nb, nsend, nrecv, me, n, shift).wait_send()
@@ -355,8 +362,8 @@
         scratch_shapes=[
             pltpu.VMEM((n, rows, width), BF16),
             pltpu.VMEM((n, ssm, width), BF16),
-            pltpu.VMEM((n, own, rows), BF16),
-            pltpu.VMEM((n, own, rows), BF16),
+            pltpu.VMEM((2, n, own, rows // 2), BF16),
+            pltpu.VMEM((2, n, own, rows // 2), BF16),
             pltpu.VMEM((n,) + norm_params.shape, BF16),
             pltpu.VMEM((n, 2, rows), F32),
             pltpu.VMEM(proj_in.shape, BF16),
@@ -370,8 +377,8 @@
             pltpu.VMEM((layers, groups, 2 * state, own // groups), F32),
             pltpu.VMEM((rows, width), BF16),
             *[pltpu.VMEM(a.shape, a.dtype) for a in args[6:]],
-            dma((5, slots)),
-            dma((5, slots)),
+            dma((7, slots)),
+            dma((7, slots)),
             dma((n - 1,)),
             dma((n - 1,)),
             dma((n - 1,)),

time: 108 us -> 120 us (1.11)
  Pallas kernels: 108 us -> 119 us
    pallas_call x1, Pallas kernels: 106 us -> 117 us  [per_device(): pl.pallas_call(functools.partial(kernel, n), out_shape=(pltpu.VMEM(tokens...]
where the time goes in v3:
time: 120 us; the launch traced here: 119 us
  Pallas kernels  119 us (99%)
    pallas_call x1, Pallas kernels, per_device(): pl.pallas_call(functools.partial(kernel, n), out_shape=(pltpu.VMEM(tokens...  117 us

profile of v3, /device:TPU:0, one launch (start us, length us, event | category | flops | bytes accessed | tf_op | source)
XLA Modules:
  0.0 119.4 jit_solution(1697191065664305449)
XLA Ops:
  0.6 117.3 %shard_map.131 = (bf16[1024,128]{1,0:T(8,128)(2,1)S(1)}, f32[2,2,2,64,1024]{4,3,2,1,0:T(8,128)S(1)}) custom-call(bf16[1024,128]{1,0:T(8,128)(2,1)} %tokens.1, f32[2,2,2,64,1024]{4,3,2,1,0:T(8,128)} %carried.1, bf16[2,32,2048]{2,1,0:T(8,128)(2,1)} %bitcast.3, bf16[2,32,2048]{2,1,0:T(8,128)(2,1)} %bitcast.4, bf16[2,512,128]{2,1,0:T(8,128)(2,1)} %proj_out.1, ...), custom_call_target="tpu_custom_call" | custom-call | tf_op jit(solution)/shard_map/pallas_call | solution.py:354
  117.9 1.4 %shard_map.132 = (bf16[1024,128]{1,0:T(8,128)(2,1)}, f32[2,2,2,64,1024]{4,3,2,1,0:T(8,128)}) custom-call(bf16[1024,128]{1,0:T(8,128)(2,1)S(1)} %get-tuple-element.4.stream, f32[2,2,2,64,1024]{4,3,2,1,0:T(8,128)S(1)} %get-tuple-element.5.fresh), custom_call_target="tpu_custom_call" | custom-call | tf_op jit(solution)/shard_map/pallas_call | solution.py:392
